TPU v7x, 32 devices: a whole 2x2x4 slice. The times are simulated.
32 devices in a mesh: ep: 8 (over z, x), tp: 4 (over y, core).
Axes of the slice: x: 2, y: 2, z: 4, core: 2. Of those that a mesh axis runs over, the one named last changes fastest.
Arguments:
- tokens: bfloat16 [8192, 2048], P(('ep', 'tp')), may hold values from -6 to 6
- norm_gain: bfloat16 [2048], replicated, may hold values from 0.099609375 to 1.8984375
- expert_ids: int32 [8192, 2], P(('ep', 'tp')), may hold values from 0 to 7, all different within a row; in each aligned block of 256 rows (0 to 255, 256 to 511, ...) at most 128 rows name the same one
- group_weight: float32 [8192], P(('ep', 'tp')), may hold values from 0.25 to 1
- expert_logit: float32 [8192, 2], P(('ep', 'tp')), may hold values from -4 to 4
- w_gate: bfloat16 [8, 2048, 1024], P('ep', None, 'tp'), may hold values from -0.125 to 0.125
- w_up: bfloat16 [8, 2048, 1024], P('ep', None, 'tp'), may hold values from -0.125 to 0.125
- w_down: bfloat16 [8, 1024, 2048], P('ep', 'tp')
- final_gain: bfloat16 [2048], P('tp'), may hold values from 0.099609375 to 1.8984375
Outputs:
- normed_out: bfloat16 [8192, 2048], P('ep', 'tp')
Inputs may be any that keep to these rules, and one draw needn't show every extreme that they name: `expert_ids`: the 2 experts of a token differ. Among the rows of one device (aligned blocks of 256 tokens) no expert is named more than 128 times, a bound that some block reaches.
All inputs are finite; a program needn't handle non-finite values.
Results may differ from a plain program's by a relative error of at most 0.0058.
Values may be sent and summed in bfloat16 or wider, within the bound.
No kernel may reach another device: no remote copies, remote signals or barrier semaphores. Data moves between devices by JAX's collectives and lax.ppermute only.
A program may use at most 128 MiB of HBM per device.

v0:
```python
import jax
import jax.numpy as jnp
from jax import lax
from jax.sharding import PartitionSpec as P

D = 2048


EPS = 1e-06


def local(
    tokens, norm_gain, expert_ids, group_weight, expert_logit, w_gate, w_up, w_down, final_gain
):
    tok_dev, width = tokens.shape
    per_token = expert_ids.shape[1]
    exp_dev = w_gate.shape[0]
    experts = exp_dev * lax.axis_size("ep")
    capacity = 2 * tok_dev * per_token // experts
    assigned = tok_dev * per_token
    tokens_f = tokens.astype(jnp.float32)
    inverse_in = lax.rsqrt(jnp.mean(tokens_f * tokens_f, axis=-1, keepdims=True) + EPS)
    normed_in = (tokens_f * inverse_in * norm_gain.astype(jnp.float32)).astype(jnp.bfloat16)
    flat_ids = expert_ids.reshape(assigned)
    onehot = (flat_ids[:, None] == jnp.arange(experts, dtype=jnp.int32)[None, :]).astype(jnp.int32)
    before = jnp.cumsum(onehot, axis=0) - onehot
    slot_rank = jnp.sum(before * onehot, axis=1)
    position = slot_rank * experts + flat_ids
    owner_row = (
        jnp.zeros((capacity * experts,), jnp.int32)
        .at[position]
        .set(jnp.arange(assigned, dtype=jnp.int32) // per_token + 1)
    )
    source = normed_in[jnp.maximum(owner_row - 1, 0)]
    outgoing = jnp.where((owner_row > 0)[:, None], source, jnp.zeros_like(source)).reshape(
        capacity, experts, width
    )
    down_whole = lax.all_gather(w_down, "tp", axis=1, tiled=True)
    gate_whole, up_whole = (
        lax.all_gather(w_gate, "tp", axis=2, tiled=True),
        lax.all_gather(w_up, "tp", axis=2, tiled=True),
    )
    incoming = lax.all_to_all(outgoing, "ep", split_axis=1, concat_axis=1, tiled=True)
    item_count = incoming.shape[0]
    senders = incoming.shape[1] // exp_dev
    arranged = incoming.reshape(item_count, senders, exp_dev, width)
    routed = arranged[:, :, 0, :].reshape(item_count * senders, width)
    gate_full = jnp.dot(routed, gate_whole[0], preferred_element_type=jnp.float32)
    up_full = jnp.dot(routed, up_whole[0], preferred_element_type=jnp.float32)
    hidden = (jax.nn.silu(gate_full) * up_full).astype(jnp.bfloat16)
    product = jnp.dot(hidden, down_whole[0], preferred_element_type=jnp.float32).astype(
        jnp.bfloat16
    )
    results = [product.reshape(item_count, senders, width)]
    answer = jnp.stack(results, axis=2).reshape(item_count, senders * exp_dev, width)
    arrived = lax.all_to_all(answer, "ep", split_axis=1, concat_axis=1, tiled=True)
    picked = arrived.reshape(capacity * experts, width)[position].reshape(tok_dev, per_token, width)
    expert_share = jnp.exp(expert_logit)
    expert_share = expert_share / jnp.sum(expert_share, axis=-1, keepdims=True)
    route_weight = group_weight[:, None] * expert_share
    mixture = tokens_f + jnp.sum(route_weight[:, :, None] * picked.astype(jnp.float32), axis=1)
    residual = mixture.astype(jnp.bfloat16)
    sliced = lax.all_to_all(residual, "tp", split_axis=1, concat_axis=0, tiled=True).astype(
        jnp.float32
    )
    squares = lax.psum(jnp.sum(sliced * sliced, axis=-1), "tp")
    inverse_out = lax.rsqrt(squares / D + EPS)
    return (sliced * inverse_out[:, None] * final_gain.astype(jnp.float32)).astype(jnp.bfloat16)


def solution(mesh):
    placed = (
        P(("ep", "tp"), None),
        P(),
        P(("ep", "tp"), None),
        P(("ep", "tp")),
        P(("ep", "tp"), None),
        P("ep", None, "tp"),
        P("ep", None, "tp"),
        P("ep", "tp", None),
        P("tp"),
    )
    return jax.shard_map(
        local, mesh=mesh, in_specs=placed, out_specs=P("ep", "tp"), check_vma=False
    )
```

profile of v0, /device:TPU:0, one launch (start us, length us, event | category | flops | bytes accessed | tf_op | source)
XLA Modules:
  0.0 325.5 jit_solution(3428466047223147058)
XLA Ops:
  6.5 0.7 all-gather.6.cloned.1.call-update
  7.3 0.7 all-gather.4.cloned.1.call-update
  8.0 0.8 copy.29
  9.0 1.1 reduce-window.6
  10.7 0.7 convert_element_type.53
  11.5 2.4 scatter_custom_fusion
  14.1 1.5 fusion.16
  15.7 0.3 fusion.18
  16.0 6.1 %gather_fusion = bf16[1024,2048]{1,0:T(8,128)(2,1)} fusion(bf16[256,2048]{1,0:T(8,128)(2,1)S(1)} %fusion.18, s32[1024]{0:T(1024)S(1)} %maximum_clamp_fusion), kind=kCustom, calls=%fused_computation | custom fusion | bytes 8392704 | tf_op jit(solution)/shard_map/gather | solution.py:34
  22.1 9.9 %copy_select_fusion = bf16[128,8,2048]{2,0,1:T(8,128)(2,1)} fusion(bf16[128,8,2048]{2,1,0:T(8,128)(2,1)} %bitcast.53, pred[128,8]{0,1:T(8,128)(4,1)S(1)} %copy.32), kind=kLoop, calls=%fused_computation.12 | loop fusion | flops 2097152 | bytes 8389632 | tf_op jit(solution)/shard_map/jit(_where)/select_n | solution.py:35
  32.0 7.3 %all-to-all-start = ((bf16[128,8,2048]{2,0,1:T(8,128)(2,1)}), bf16[128,8,2048]{2,0,1:T(8,128)(2,1)}, u32[]{:S(2)}, u32[]{:S(2)}) async-start(bf16[128,8,2048]{2,0,1:T(8,128)(2,1)} %copy_select_fusion), calls=%async_computation | async-start | bytes 8388608 | tf_op jit(solution)/shard_map/all_to_all | solution.py:43
  39.3 0.2 all-gather.8.cloned.1.call-start
  39.5 0.5 all-gather.8.cloned.1.call-update
  40.0 6.7 %all-gather.6.cloned.1.call-done = bf16[1,2048,1024]{2,1,0:T(8,128)(2,1)} async-done(((bf16[1,2048,256]{2,1,0:T(8,128)(2,1)}), bf16[1,2048,1024]{2,1,0:T(8,128)(2,1)}) %all-gather.6.cloned.1.call-update) | async-done | bytes 4194320 | tf_op jit(solution)/shard_map/all_gather | solution.py:41
  46.7 85.9 %all-to-all-done = bf16[128,8,2048]{2,0,1:T(8,128)(2,1)} async-done(((bf16[128,8,2048]{2,0,1:T(8,128)(2,1)}), bf16[128,8,2048]{2,0,1:T(8,128)(2,1)}, u32[]{:S(2)}, u32[]{:S(2)}) %all-to-all-start) | async-done | bytes 4194336 | tf_op jit(solution)/shard_map/all_to_all | solution.py:43
  132.5 10.3 %fusion.2 = f32[1024,1024]{1,0:T(8,128)} fusion(bf16[1,2048,1024]{2,1,0:T(8,128)(2,1)} %all-gather.6.cloned.1.call-done, bf16[128,8,2048]{2,0,1:T(8,128)(2,1)} %all-to-all-done), kind=kOutput, calls=%fused_computation.5 | convolution fusion | flops 4294967296 | bytes 12582912 | tf_op jit(solution)/shard_map/dot_general | solution.py:49
  142.9 11.4 %multiply_convert_fusion = bf16[1024,1024]{1,0:T(8,128)(2,1)} fusion(f32[1024,1024]{1,0:T(8,128)} %fusion.2, bf16[1,2048,1024]{2,1,0:T(8,128)(2,1)} %all-gather.4.cloned.1.call-done, bf16[128,8,2048]{2,0,1:T(8,128)(2,1)} %all-to-all-done), kind=kOutput, calls=%fused_computation.15 | convolution fusion | flops 4301258752 | bytes 14680064 | tf_op jit(solution)/shard_map/dot_general | solution.py:48
  154.3 7.3 %convert_bitcast_fusion = bf16[128,8,2048]{2,1,0:T(8,128)(2,1)S(1)} fusion(bf16[1024,1024]{1,0:T(8,128)(2,1)} %multiply_convert_fusion, bf16[1,1024,2048]{2,1,0:T(8,128)(2,1)} %all-gather.8.cloned.1.call-done), kind=kOutput, calls=%fused_computation.14 | convolution fusion | flops 4297064448 | bytes 10485760 | tf_op jit(solution)/shard_map/dot_general | solution.py:51
  161.6 4.5 %copy.35 = bf16[128,8,2048]{2,0,1:T(8,128)(2,1)} copy(bf16[128,8,2048]{2,1,0:T(8,128)(2,1)S(1)} %convert_bitcast_fusion) | data formatting | bytes 8388608 | tf_op jit(solution)/shard_map/reshape;stack;reshape | solution.py:55
  166.1 4.7 %all-to-all-start.1 = ((bf16[128,8,2048]{2,0,1:T(8,128)(2,1)}), bf16[128,8,2048]{2,0,1:T(8,128)(2,1)}, u32[]{:S(2)}, u32[]{:S(2)}) async-start(bf16[128,8,2048]{2,0,1:T(8,128)(2,1)} %copy.35), calls=%async_computation.1 | async-start | bytes 8388608 | tf_op jit(solution)/shard_map/all_to_all | solution.py:56
  171.0 92.4 %all-to-all-done.1 = bf16[128,8,2048]{2,0,1:T(8,128)(2,1)} async-done(((bf16[128,8,2048]{2,0,1:T(8,128)(2,1)}), bf16[128,8,2048]{2,0,1:T(8,128)(2,1)}, u32[]{:S(2)}, u32[]{:S(2)}) %all-to-all-start.1) | async-done | bytes 4194336 | tf_op jit(solution)/shard_map/all_to_all | solution.py:56
  263.3 6.5 %copy.56 = bf16[128,8,2048]{2,1,0:T(8,128)(2,1)} copy(bf16[128,8,2048]{2,0,1:T(8,128)(2,1)} %all-to-all-done.1) | data formatting | bytes 8388608 | tf_op jit(solution)/shard_map/all_to_all | solution.py:56
  269.8 8.0 %gather_fusion.1 = bf16[512,2048]{1,0:T(8,128)(2,1)} fusion(bf16[1024,2048]{1,0:T(8,128)(2,1)} %bitcast.52, s32[1024]{0:T(1024)S(1)} %pad_clamp_fusion), kind=kCustom, calls=%fused_computation.1 | custom fusion | bytes 4196352 | tf_op jit(solution)/shard_map/gather | solution.py:57
  277.7 5.4 %reshape.85 = f32[256,2,2048]{2,1,0:T(2,128)} reshape(bf16[512,2048]{1,0:T(8,128)(2,1)} %gather_fusion.1) | data formatting | bytes 6291456 | tf_op jit(solution)/shard_map/convert_element_type | solution.py:61
  283.2 8.9 %multiply_reduce_fusion = f32[256,2048]{1,0:T(8,128)S(1)} fusion(f32[256,2,2048]{2,1,0:T(2,128)} %reshape.85, f32[256,2]{1,0:T(8,128)S(1)} %copy.28), kind=kLoop, calls=%fused_computation.13 | loop fusion | flops 1572864 | bytes 6293504 | tf_op jit(solution)/shard_map/reduce_sum | solution.py:61
  292.1 0.3 fusion.19
  292.4 1.1 copy.57
  293.5 3.5 %all-to-all-start.2 = ((bf16[256,4,512]{2,0,1:T(8,128)(2,1)}), bf16[256,4,512]{2,0,1:T(8,128)(2,1)S(1)}, u32[]{:S(2)}, u32[]{:S(2)}) async-start(bf16[256,4,512]{2,0,1:T(8,128)(2,1)} %bitcast.51), calls=%async_computation.2 | async-start | bytes 2097152 | tf_op jit(solution)/shard_map/all_to_all | solution.py:63
  297.0 14.4 %all-to-all-done.2 = bf16[256,4,512]{2,0,1:T(8,128)(2,1)S(1)} async-done(((bf16[256,4,512]{2,0,1:T(8,128)(2,1)}), bf16[256,4,512]{2,0,1:T(8,128)(2,1)S(1)}, u32[]{:S(2)}, u32[]{:S(2)}) %all-to-all-start.2) | async-done | bytes 1048608 | tf_op jit(solution)/shard_map/all_to_all | solution.py:63
  311.4 0.3 multiply_reduce_fusion.1
  311.9 5.8 %psum.7 = f32[1024]{0:T(1024)S(1)} all-reduce(f32[1024]{0:T(1024)S(1)} %bitcast.57), channel_id=1, replica_groups=mesh['ep'=8,'tp'=4] {'tp'}, use_global_device_ids=true, to_apply=%region_8.9 | all-reduce | flops 1024 | bytes 8192 | tf_op jit(solution)/shard_map/psum | solution.py:66
  317.7 1.3 fusion.21
  (37 shorter events, 1.4 us)
Async XLA Ops:
  6.5 9.1 %copy-start = (bf16[256,2048]{1,0:T(8,128)(2,1)S(1)}, bf16[256,2048]{1,0:T(8,128)(2,1)}, u32[]{:S(2)}) copy-start(bf16[256,2048]{1,0:T(8,128)(2,1)} %param.9) | copy-start | bytes 3145732
  6.5 40.2 %all-gather.6.cloned.1.call-start = ((), (), s32[]{:S(2)}) async-start(), calls=%async_computation.4 | async-start | bytes 5242880 | tf_op jit(solution)/shard_map/all_gather | solution.py:41
  7.3 135.6 %all-gather.4.cloned.1.call-start = ((), (), s32[]{:S(2)}) async-start(), calls=%async_computation.3 | async-start | bytes 5242880 | tf_op jit(solution)/shard_map/all_gather | solution.py:40
  32.0 100.6 %all-to-all-start = ((bf16[128,8,2048]{2,0,1:T(8,128)(2,1)}), bf16[128,8,2048]{2,0,1:T(8,128)(2,1)}, u32[]{:S(2)}, u32[]{:S(2)}) async-start(bf16[128,8,2048]{2,0,1:T(8,128)(2,1)} %copy_select_fusion), calls=%async_computation | async-start | bytes 8388608 | tf_op jit(solution)/shard_map/all_to_all | solution.py:43
  39.3 115.0 %all-gather.8.cloned.1.call-start = ((), (), s32[]{:S(2)}) async-start(), calls=%async_computation.5 | async-start | bytes 5242880 | tf_op jit(solution)/shard_map/all_gather | solution.py:38
  166.1 4.7 %copy-start.1 = (f32[256,2]{0,1:T(2,128)S(1)}, f32[256,2]{0,1:T(2,128)}, u32[]{:S(2)}) copy-start(f32[256,2]{0,1:T(2,128)} %param.13) | copy-start | bytes 6148
  166.1 4.7 %copy-start.3 = (f32[256]{0:T(256)S(1)}, f32[256]{0:T(256)}, u32[]{:S(2)}) copy-start(f32[256]{0:T(256)} %param.12) | copy-start | bytes 3076
  166.1 97.2 %all-to-all-start.1 = ((bf16[128,8,2048]{2,0,1:T(8,128)(2,1)}), bf16[128,8,2048]{2,0,1:T(8,128)(2,1)}, u32[]{:S(2)}, u32[]{:S(2)}) async-start(bf16[128,8,2048]{2,0,1:T(8,128)(2,1)} %copy.35), calls=%async_computation.1 | async-start | bytes 8388608 | tf_op jit(solution)/shard_map/all_to_all | solution.py:56
  292.1 4.9 %copy-start.2 = (bf16[512]{0:T(512)(128)(2,1)S(1)}, bf16[512]{0:T(512)(128)(2,1)}, u32[]{:S(2)}) copy-start(bf16[512]{0:T(512)(128)(2,1)} %param.17) | copy-start | bytes 3076
  293.5 17.9 %all-to-all-start.2 = ((bf16[256,4,512]{2,0,1:T(8,128)(2,1)}), bf16[256,4,512]{2,0,1:T(8,128)(2,1)S(1)}, u32[]{:S(2)}, u32[]{:S(2)}) async-start(bf16[256,4,512]{2,0,1:T(8,128)(2,1)} %bitcast.51), calls=%async_computation.2 | async-start | bytes 2097152 | tf_op jit(solution)/shard_map/all_to_all | solution.py:63
Sparse Core Ops, SparseCore 0:
  8.9 37.7 all-gather.5
  48.2 34.9 all-gather.3
  84.8 34.4 all-gather.7
where the time goes:
time: 326 us; the launch traced here: 325 us
  waiting for transfers between devices  201 us (62%)
  local copies, waits for them, and re-layouts  35.9 us (11%)
  matrix products  29 us (9%)
  other arithmetic  24.6 us (8%)
  starting transfers between devices  15.7 us (5%)
  between operations  13.3 us (4%)
  blocking collectives  5.75 us (2%)
    all_to_all x1, waiting for transfers between devices, local(): lax.all_to_all(answer, 'ep', split_axis=1, concat_axis=1, tiled=True)  92.4 us
    all_to_all x1, waiting for transfers between devices, local(): lax.all_to_all(outgoing, 'ep', split_axis=1, concat_axis=1, tiled=True)  85.9 us
    all_to_all x1, waiting for transfers between devices, local(): lax.all_to_all(residual, 'tp', split_axis=1, concat_axis=0, tiled=True)  14.4 us
    dot_general x1, matrix products, local(): jnp.dot(routed, gate_whole[0], preferred_element_type=jnp.float32)  11.4 us
    dot_general x1, matrix products, local(): up_full = jnp.dot(routed, up_whole[0], preferred_element_type=jnp.float32)  10.3 us
    select_n x1, other arithmetic, local(): jnp.where((owner_row > 0)[:, None], source, jnp.zeros_like(source))  9.92 us
    reduce_sum x1, other arithmetic, local(): jnp.sum(route_weight[:, :, None] * picked.astype(jnp.float32), axis=1)  8.89 us
    gather x1, local copies, waits for them, and re-layouts, local(): arrived.reshape(capacity * experts, width)[position]  7.96 us
  transfers between devices with their start and end apart: 6, of which 4 were waited for; matrix products, arithmetic and copies ran while one was open for 14% of the time, Pallas kernels for 0%

commit v1 on v0

--- a/solution.py
+++ b/solution.py
@@ -1,15 +1,26 @@
+import functools
+
 import jax
 import jax.numpy as jnp
 from jax import lax
+from jax.experimental import pallas as pl
+from jax.experimental.pallas import tpu as pltpu
 from jax.sharding import PartitionSpec as P
 
 D = 2048
 
 
 EPS = 1e-06
-
-
-def local(
+BF16, F32 = jnp.bfloat16, jnp.float32
+LEVELS, COLUMNS = 4, 2
+TP = 4
+ANY = pl.BlockSpec(memory_space=pl.ANY)
+SMEM = pl.BlockSpec(memory_space=pltpu.SMEM)
+VMEM = pl.BlockSpec(memory_space=pltpu.VMEM)
+PARAMS = pltpu.CompilerParams(vmem_limit_bytes=56 * 1024 * 1024)
+
+
+def flat_plan(
     tokens, norm_gain, expert_ids, group_weight, expert_logit, w_gate, w_up, w_down, final_gain
 ):
     tok_dev, width = tokens.shape
@@ -68,6 +79,296 @@
     return (sliced * inverse_out[:, None] * final_gain.astype(jnp.float32)).astype(jnp.bfloat16)
 
 
+def expert_rows(meta, expert, slots, weighted):
+    tok = meta.shape[1]
+    first, second = meta[0:1, :] == expert, meta[1:2, :] == expert
+    member = jnp.where(first | second, 1.0, 0.0).astype(F32)
+    earlier = (
+        lax.broadcasted_iota(jnp.int32, (tok, tok), 0)
+        < lax.broadcasted_iota(jnp.int32, (tok, tok), 1)
+    ).astype(F32)
+    rank = jnp.dot(
+        jnp.broadcast_to(member, (8, tok)).astype(BF16),
+        earlier.astype(BF16),
+        preferred_element_type=F32,
+    )[0:1, :]
+    key = jnp.where(member > 0.0, rank, -1.0)
+    here = key == lax.broadcasted_iota(jnp.int32, (slots, tok), 0).astype(F32)
+    if not weighted:
+        return jnp.where(here, 1.0, 0.0).astype(F32)
+    weight = jnp.where(first, meta[2:3, :], jnp.where(second, meta[3:4, :], 0.0))
+    return jnp.where(here, weight, 0.0)
+
+
+def pick_body(pos, table, gain, *refs, count, slots):
+    blocks = refs[:count]
+    own_out, side_out, block, sem = refs[count:]
+    for number in range(count):
+
+        @pl.when(pos[0] == number)
+        def _():
+            copy = pltpu.make_async_copy(blocks[number], block, sem)
+            copy.start()
+            copy.wait()
+
+    meta = table[pos[1]]
+    width = block.shape[1]
+    step = 32
+
+    def norm(index, carry):
+        rows = pl.ds(pl.multiple_of(index * step, step), step)
+        values = block[rows, :].astype(F32)
+        inverse = lax.rsqrt(jnp.mean(values * values, axis=-1, keepdims=True) + EPS)
+        block[rows, :] = (values * inverse * gain[...].astype(F32)).astype(BF16)
+        return carry
+
+    lax.fori_loop(0, block.shape[0] // step, norm, 0)
+    for expert, out in ((pos[2], own_out), (pos[3], side_out)):
+        chosen = expert_rows(meta, expert.astype(F32), slots, False).astype(BF16)
+        for start in range(0, width, 512):
+            out[:, start : start + 512] = jnp.dot(
+                chosen, block[:, start : start + 512], preferred_element_type=F32
+            ).astype(BF16)
+
+
+def pick(pos, table, gain, blocks, slots):
+    rows = jax.ShapeDtypeStruct((slots, blocks[0].shape[1]), BF16)
+    return pl.pallas_call(
+        functools.partial(pick_body, count=len(blocks), slots=slots),
+        in_specs=[SMEM, VMEM, VMEM] + [ANY] * len(blocks),
+        out_specs=[VMEM, VMEM],
+        out_shape=[rows, rows],
+        scratch_shapes=[pltpu.VMEM(blocks[0].shape, BF16), pltpu.SemaphoreType.DMA],
+        compiler_params=PARAMS,
+        name="pick",
+    )(pos, table, gain, *blocks)
+
+
+def experts_body(*refs, count, pieces):
+    inputs = refs[:count]
+    gates = refs[count : count + pieces]
+    ups = refs[count + pieces : count + 2 * pieces]
+    downs = refs[count + 2 * pieces : count + 3 * pieces]
+    outs = refs[count + 3 * pieces : 2 * count + 3 * pieces]
+    rows, gate, up, down, hidden, row_sem, weight_sem = refs[2 * count + 3 * pieces :]
+    part = gate.shape[2]
+    slots = inputs[0].shape[0]
+    width = rows.shape[1]
+    row_copies = [
+        pltpu.make_async_copy(ref, rows.at[pl.ds(n * slots, slots)], row_sem.at[n])
+        for n, ref in enumerate(inputs)
+    ]
+    copies = []
+    for n in range(pieces):
+        copies.append(pltpu.make_async_copy(gates[n].at[0], gate.at[n], weight_sem.at[n, 0]))
+        copies.append(pltpu.make_async_copy(ups[n].at[0], up.at[n], weight_sem.at[n, 1]))
+    for n in range(pieces):
+        copies.append(
+            pltpu.make_async_copy(
+                downs[n].at[0], down.at[pl.ds(n * part, part)], weight_sem.at[n, 2]
+            )
+        )
+    for copy in row_copies + copies:
+        copy.start()
+    for copy in row_copies:
+        copy.wait()
+    for n in range(pieces):
+        copies[2 * n].wait()
+        copies[2 * n + 1].wait()
+        gated = jnp.dot(rows[...], gate[n], preferred_element_type=F32)
+        upper = jnp.dot(rows[...], up[n], preferred_element_type=F32)
+        hidden[:, n * part : (n + 1) * part] = (
+            gated / (1.0 + jnp.exp(-gated)) * upper
+        ).astype(BF16)
+    for n in range(pieces):
+        copies[2 * pieces + n].wait()
+    for start in range(0, width, 512):
+        product = jnp.dot(
+            hidden[...], down[:, start : start + 512], preferred_element_type=F32
+        ).astype(BF16)
+        for n, out in enumerate(outs):
+            out[:, start : start + 512] = product[n * slots : (n + 1) * slots]
+
+
+def experts(inputs, gates, ups, downs):
+    count, pieces = len(inputs), len(gates)
+    slots, width = inputs[0].shape
+    part = gates[0].shape[2]
+    total = count * slots
+    return pl.pallas_call(
+        functools.partial(experts_body, count=count, pieces=pieces),
+        in_specs=[ANY] * (count + 3 * pieces),
+        out_specs=[VMEM] * count,
+        out_shape=[jax.ShapeDtypeStruct((slots, width), BF16)] * count,
+        scratch_shapes=[
+            pltpu.VMEM((total, width), BF16),
+            pltpu.VMEM((pieces, width, part), BF16),
+            pltpu.VMEM((pieces, width, part), BF16),
+            pltpu.VMEM((pieces * part, width), BF16),
+            pltpu.VMEM((total, pieces * part), BF16),
+            pltpu.SemaphoreType.DMA((count,)),
+            pltpu.SemaphoreType.DMA((pieces, 3)),
+        ],
+        compiler_params=PARAMS,
+        cost_estimate=pl.CostEstimate(
+            flops=6 * total * width * pieces * part,
+            bytes_accessed=6 * width * pieces * part + 4 * total * width,
+            transcendentals=total * pieces * part,
+        ),
+        name="experts",
+    )(*inputs, *gates, *ups, *downs)
+
+
+def mix_body(pos, table, own, side, *refs):
+    out = refs[-1]
+    slots, width = own.shape
+    meta = table[pos[1]]
+    parts = []
+    for expert, rows in ((pos[2], own), (pos[3], side)):
+        weights = expert_rows(meta, expert.astype(F32), slots, True).T
+        high = weights.astype(BF16)
+        low = (weights - high.astype(F32)).astype(BF16)
+        parts.append((high, low, rows))
+    for start in range(0, width, 512):
+        total = 0.0
+        for high, low, rows in parts:
+            values = rows[:, start : start + 512]
+            total = total + jnp.dot(high, values, preferred_element_type=F32)
+            total = total + jnp.dot(low, values, preferred_element_type=F32)
+        for more in refs[:-1]:
+            total = total + more[:, start : start + 512].astype(F32)
+        out[:, start : start + 512] = total.astype(out.dtype)
+
+
+def mix(pos, table, own, side, more, dtype):
+    tok = table.shape[2]
+    return pl.pallas_call(
+        mix_body,
+        in_specs=[SMEM] + [VMEM] * (3 + len(more)),
+        out_specs=VMEM,
+        out_shape=jax.ShapeDtypeStruct((tok, own.shape[1]), dtype),
+        compiler_params=PARAMS,
+        name="mix",
+    )(pos, table, own, side, *more)
+
+
+def close_body(base, first, second, gain, out):
+    step = 32
+
+    def norm(index, carry):
+        rows = pl.ds(pl.multiple_of(index * step, step), step)
+        values = base[rows, :] + first[rows, :].astype(F32) + second[rows, :].astype(F32)
+        values = values.astype(BF16).astype(F32)
+        inverse = lax.rsqrt(jnp.mean(values * values, axis=-1, keepdims=True) + EPS)
+        out[rows, :] = (values * inverse * gain[...].astype(F32)).astype(BF16)
+        return carry
+
+    lax.fori_loop(0, out.shape[0] // step, norm, 0)
+
+
+def close(base, first, second, gain):
+    return pl.pallas_call(
+        close_body,
+        in_specs=[VMEM] * 4,
+        out_specs=VMEM,
+        out_shape=jax.ShapeDtypeStruct(base.shape, BF16),
+        compiler_params=PARAMS,
+        name="close",
+    )(base, first, second, gain)
+
+
+def hops(moves):
+    return [
+        (a * COLUMNS + col, b * COLUMNS + col) for a, b in moves for col in range(COLUMNS)
+    ]
+
+
+def staged_plan(
+    tokens, norm_gain, expert_ids, group_weight, expert_logit, w_gate, w_up, w_down, final_gain
+):
+    tok_dev, width = tokens.shape
+    per_token = expert_ids.shape[1]
+    ranks = lax.axis_size("ep")
+    slots = 2 * tok_dev * per_token // ranks
+    me = lax.axis_index("ep")
+    level = me // COLUMNS
+    lower = level < LEVELS // 2
+
+    def line(value, *moves):
+        return lax.ppermute(value, "ep", hops(moves))
+
+    def across(value):
+        return lax.ppermute(value, "ep", [(n, n ^ 1) for n in range(ranks)])
+
+    def twin(value, flip):
+        return lax.ppermute(value, "tp", [(n, n ^ flip) for n in range(TP)])
+
+    expert_share = jnp.exp(expert_logit)
+    expert_share = expert_share / jnp.sum(expert_share, axis=-1, keepdims=True)
+    route_weight = group_weight[:, None] * expert_share
+    meta = jnp.concatenate(
+        [
+            expert_ids.T.astype(F32),
+            route_weight.T,
+            jnp.zeros((8 - 2 * per_token, tok_dev), F32),
+        ]
+    )
+    table = lax.all_to_all(
+        jnp.broadcast_to(meta[None], (ranks,) + meta.shape), "ep", 0, 0, tiled=True
+    )
+    gain_out = lax.all_to_all(
+        jnp.broadcast_to(final_gain[None], (TP,) + final_gain.shape), "tp", 0, 0, tiled=True
+    ).reshape(1, width)
+    gain_in = norm_gain.reshape(1, width)
+
+    up1 = line(tokens, (0, 1), (1, 2), (2, 3))
+    down1 = line(tokens, (3, 2), (2, 1), (1, 0))
+    weights = [[w, None, twin(w, 2), None] for w in (w_gate, w_up, w_down)]
+    for pieces in weights:
+        pieces[1] = twin(pieces[0], 1)
+        pieces[3] = twin(pieces[2], 1)
+    up2 = line(up1, (1, 2), (2, 3))
+    down2 = line(down1, (2, 1), (1, 0))
+    up3 = line(up2, (2, 3))
+    down3 = line(down2, (1, 0))
+
+    def slot(which, source):
+        source = source * COLUMNS + me % COLUMNS
+        return jnp.stack([which, source, me, me ^ 1]).astype(jnp.int32)
+
+    far = 1 - lower.astype(jnp.int32)
+    sign = 1 - 2 * far
+    places = [
+        slot(0 * me, level),
+        slot(far, level + sign),
+        slot(far, level + 2 * sign),
+        slot(level, (LEVELS - 1) * (1 - level % 2)),
+    ]
+    blocks = [(tokens,), (down1, up1), (down2, up2), (down3, up1, down1, up3)]
+    picked = [pick(p, table, gain_in, b, slots) for p, b in zip(places, blocks)]
+    rows = [(own, across(side)) for own, side in picked]
+    near = experts([r for pair in rows[:3] for r in pair], *weights)
+    last = experts(list(rows[3]), *weights)
+    done = [(near[0], near[1]), (near[2], near[3]), (near[4], near[5]), (last[0], last[1])]
+    back = [(own, across(side)) for own, side in reversed(done)][::-1]
+
+    sums3 = mix(places[3], table, *back[3], (), BF16)
+    got1 = line(sums3, (0, 1), (3, 2))
+    sums2 = mix(places[2], table, *back[2], (got1,), BF16)
+    got_up, got_down = line(sums2, (0, 1), (1, 2)), line(sums2, (3, 2), (2, 1))
+    sums1 = mix(places[1], table, *back[1], (), BF16)
+    base = mix(places[0], table, *back[0], (tokens,), F32)
+
+    def join(level_of_last, got):
+        mine = jnp.where(level == level_of_last, sums3, sums1)
+        return (mine.astype(F32) + got.astype(F32)).astype(BF16)
+
+    first = line(join(2, got_up), (0, 1), (1, 2), (2, 3))
+    second = line(join(1, got_down), (3, 2), (2, 1), (1, 0))
+    normed = close(base, first, second, gain_out)
+    return lax.all_to_all(normed, "tp", split_axis=1, concat_axis=0, tiled=True)
+
+
 def solution(mesh):
     placed = (
         P(("ep", "tp"), None),
@@ -80,6 +381,11 @@
         P("ep", "tp", None),
         P("tp"),
     )
+    line = mesh.shape["ep"] == LEVELS * COLUMNS and mesh.shape["tp"] == TP
     return jax.shard_map(
-        local, mesh=mesh, in_specs=placed, out_specs=P("ep", "tp"), check_vma=False
-    )
+        staged_plan if line else flat_plan,
+        mesh=mesh,
+        in_specs=placed,
+        out_specs=P("ep", "tp"),
+        check_vma=False,
+    )

time: 326 us -> 267 us (0.82)
  waiting for transfers between devices: 201 us -> 109 us
  Pallas kernels: 0 us -> 66.4 us
  starting transfers between devices: 15.7 us -> 46 us
  matrix products: 29 us -> 0 us
  local copies, waits for them, and re-layouts: 35.9 us -> 11.4 us
  blocking collectives: 5.75 us -> 23.4 us
  other arithmetic: 24.6 us -> 8.68 us
  between operations: 13.3 us -> 0.3 us
    all_to_all x3 -> x1, waiting for transfers between devices: 193 us -> 4.96 us  [staged_plan(): lax.all_to_all(jnp.broadcast_to(meta[None], (ranks,) + meta.shape), 'ep',...]
    ppermute x0 -> x28, waiting for transfers between devices: none -> 104 us  [the longest x11 47 us: line(): return lax.ppermute(value, 'ep', hops(moves))]
    pallas_call x0 -> x11, Pallas kernels: none -> 66.4 us  [the longest x2 27.5 us: experts(): pl.pallas_call(functools.partial(experts_body, count=count, pieces=pieces...]
    ppermute x0 -> x28, starting transfers between devices: none -> 38.7 us  [the longest x11 25.3 us: line(): return lax.ppermute(value, 'ep', hops(moves))]
    dot_general x3 -> x0, matrix products: 29 us -> none  [the longest x1 11.4 us: local(): jnp.dot(routed, gate_whole[0], preferred_element_type=jnp.float32)]
    all_to_all x0 -> x2, blocking collectives: none -> 23.4 us  [the longest x1 17 us: staged_plan(): return lax.all_to_all(normed, 'tp', split_axis=1, concat_axis=0, tiled=True)]
    gather x2 -> x0, local copies, waits for them, and re-layouts: 14 us -> none  [the longest x1 7.96 us: local(): arrived.reshape(capacity * experts, width)[position]]
    reduce_sum x5 -> x1, other arithmetic: 10.8 us -> 0.7 us  [staged_plan(): expert_share = expert_share / jnp.sum(expert_share, axis=-1, keepdims=True)]
  transfers between devices with their start and end apart: 6 -> 29, of which waited for: 4 -> 15; matrix products, arithmetic and copies ran while one was open for 14% -> 3% of each run, Pallas kernels for 0% -> 22%
where the time goes in v1:
time: 267 us; the launch traced here: 265 us
  waiting for transfers between devices  109 us (41%)
  Pallas kernels  66.4 us (25%)
  starting transfers between devices  46 us (17%)
  blocking collectives  23.4 us (9%)
  local copies, waits for them, and re-layouts  11.4 us (4%)
  other arithmetic  8.68 us (3%)
    ppermute x11, waiting for transfers between devices, line(): return lax.ppermute(value, 'ep', hops(moves))  47 us
    ppermute x8, waiting for transfers between devices, across(): return lax.ppermute(value, 'ep', [(n, n ^ 1) for n in range(ranks)])  38 us
    pallas_call x2, Pallas kernels, experts(): pl.pallas_call(functools.partial(experts_body, count=count, pieces=pieces...  27.5 us
    ppermute x11, starting transfers between devices, line(): return lax.ppermute(value, 'ep', hops(moves))  25.3 us
    ppermute x9, waiting for transfers between devices, twin(): return lax.ppermute(value, 'tp', [(n, n ^ flip) for n in range(TP)])  19.1 us
    pallas_call x4, Pallas kernels, pick(): pl.pallas_call(functools.partial(pick_body, count=len(blocks), slots=slot...  18.7 us
    all_to_all x1, blocking collectives, staged_plan(): return lax.all_to_all(normed, 'tp', split_axis=1, concat_axis=0, tiled=True)  17 us
    pallas_call x4, Pallas kernels, mix(): pl.pallas_call(mix_body, in_specs=[SMEM] + [VMEM] * (3 + len(more)), out_...  15.7 us
  transfers between devices with their start and end apart: 29, of which 15 were waited for; matrix products, arithmetic and copies ran while one was open for 3% of the time, Pallas kernels for 22%

profile of v1, /device:TPU:0, one launch (start us, length us, event | category | flops | bytes accessed | tf_op | source)
XLA Modules:
  0.0 265.4 jit_solution(7274924625063172016)
XLA Ops:
  1.3 5.7 %collective-permute-start.2 = (bf16[256,2048]{1,0:T(8,128)(2,1)}, bf16[256,2048]{1,0:T(8,128)(2,1)S(1)}, u32[]{:S(2)}, u32[]{:S(2)}) collective-permute-start(bf16[256,2048]{1,0:T(8,128)(2,1)} %refs_0_.3), channel_id=1, source_target_pairs={{0,8},{4,12},{8,16},{12,20},{16,24},{20,28},{1,9},{5,13},{9,17},{1... | collective-permute-start | bytes 3145736 | tf_op jit(solution)/shard_map/ppermute | solution.py:298
  7.0 2.0 collective-permute-start.8
  9.0 19.3 %collective-permute-done.1.refs_0_.refs_2_ = bf16[256,2048]{1,0:T(8,128)(2,1)S(1)} collective-permute-done((bf16[256,2048]{1,0:T(8,128)(2,1)}, bf16[256,2048]{1,0:T(8,128)(2,1)S(1)}, u32[]{:S(2)}, u32[]{:S(2)}) %collective-permute-start.1) | collective-permute-done | bytes 1048608 | tf_op jit(solution)/shard_map/ppermute | solution.py:298
  30.4 1.7 collective-permute-start.11
  33.6 21.0 %collective-permute-done.4.refs_0_ = bf16[256,2048]{1,0:T(8,128)(2,1)S(1)} collective-permute-done((bf16[256,2048]{1,0:T(8,128)(2,1)S(1)}, bf16[256,2048]{1,0:T(8,128)(2,1)S(1)}, u32[]{:S(2)}, u32[]{:S(2)}) %collective-permute-start.4) | collective-permute-done | bytes 1048608 | tf_op jit(solution)/shard_map/ppermute | solution.py:298
  59.7 19.1 %collective-permute-done.14.refs_16_.refs_12_ = bf16[1,256,2048]{2,1,0:T(8,128)(2,1)} collective-permute-done((bf16[1,256,2048]{2,1,0:T(8,128)(2,1)}, bf16[1,256,2048]{2,1,0:T(8,128)(2,1)}, u32[]{:S(2)}, u32[]{:S(2)}) %collective-permute-start.14) | collective-permute-done | bytes 1048608 | tf_op jit(solution)/shard_map/ppermute | solution.py:304
  82.1 7.3 %all-to-all-start = ((f32[8,8,256]{2,1,0:T(8,128)}), f32[8,8,256]{2,1,0:T(8,128)S(1)}, u32[]{:S(2)}, u32[]{:S(2)}) async-start(f32[8,8,256]{2,1,0:T(8,128)} %broadcast_in_dim.7), calls=%async_computation | async-start | bytes 131072 | tf_op jit(solution)/shard_map/all_to_all | solution.py:316
  91.3 5.0 %all-to-all-done.table = f32[8,8,256]{2,1,0:T(8,128)S(1)} async-done(((f32[8,8,256]{2,1,0:T(8,128)}), f32[8,8,256]{2,1,0:T(8,128)S(1)}, u32[]{:S(2)}, u32[]{:S(2)}) %all-to-all-start) | async-done | bytes 65568 | tf_op jit(solution)/shard_map/all_to_all | solution.py:316
  96.9 4.7 %pick.7 = (bf16[128,2048]{1,0:T(8,128)(2,1)}, bf16[128,2048]{1,0:T(8,128)(2,1)}) custom-call(s32[4]{0:T(128)} %add_add_fusion.3.pos, f32[8,8,256]{2,1,0:T(8,128)} %copy-done, bf16[1,2048]{1,0:T(2,128)(2,1)} %reshape.19.gain, bf16[256,2048]{1,0:T(8,128)(2,1)} %copy-done.4, bf16[256,2048]{1,0:T(8,128)(2,1)} %copy-done.2, bf16[256,2048]{1,0:T(8,128)(2,1)} %copy-done.1, ...), custom_call_target="tpu_custom_call" | custom-call | tf_op jit(solution)/shard_map/pick/pallas_call | solution.py:136
  104.0 4.7 %pick.4 = (bf16[128,2048]{1,0:T(8,128)(2,1)}, bf16[128,2048]{1,0:T(8,128)(2,1)}) custom-call(s32[4]{0:T(128)} %add_add_fusion.pos, f32[8,8,256]{2,1,0:T(8,128)} %copy-done, bf16[1,2048]{1,0:T(2,128)(2,1)} %reshape.19.gain, bf16[256,2048]{1,0:T(8,128)(2,1)} %refs_0_.3), custom_call_target="tpu_custom_call" | custom-call | tf_op jit(solution)/shard_map/pick/pallas_call | solution.py:136
  110.4 6.3 %collective-permute-done.19.refs_1_ = bf16[128,2048]{1,0:T(8,128)(2,1)S(1)} collective-permute-done((bf16[128,2048]{1,0:T(8,128)(2,1)}, bf16[128,2048]{1,0:T(8,128)(2,1)S(1)}, u32[]{:S(2)}, u32[]{:S(2)}) %collective-permute-start.19) | collective-permute-done | bytes 524320 | tf_op jit(solution)/shard_map/ppermute | solution.py:301
  117.5 9.8 %experts.3 = (bf16[128,2048]{1,0:T(8,128)(2,1)}, bf16[128,2048]{1,0:T(8,128)(2,1)}) custom-call(bf16[128,2048]{1,0:T(8,128)(2,1)} %get-tuple-element.29.refs_0_, bf16[128,2048]{1,0:T(8,128)(2,1)} %copy-done.13, bf16[1,2048,256]{2,1,0:T(8,128)(2,1)} %refs_2_.1, bf16[1,2048,256]{2,1,0:T(8,128)(2,1)} %collective-permute-done.7.refs_7_.refs_3_, ...), custom_call_target="tpu_custom_call" | custom-call | flops 3221225472 | bytes 14680064 | tf_op jit(solution)/shard_map/experts/pallas_call | solution.py:198
  127.8 4.7 %pick.5 = (bf16[128,2048]{1,0:T(8,128)(2,1)}, bf16[128,2048]{1,0:T(8,128)(2,1)}) custom-call(s32[4]{0:T(128)} %add_add_fusion.1.pos, f32[8,8,256]{2,1,0:T(8,128)} %copy-done, bf16[1,2048]{1,0:T(2,128)(2,1)} %reshape.19.gain, bf16[256,2048]{1,0:T(8,128)(2,1)} %copy-done.1, bf16[256,2048]{1,0:T(8,128)(2,1)} %copy-done.2), custom_call_target="tpu_custom_call" | custom-call | tf_op jit(solution)/shard_map/pick/pallas_call | solution.py:136
  134.2 4.7 %pick.6 = (bf16[128,2048]{1,0:T(8,128)(2,1)}, bf16[128,2048]{1,0:T(8,128)(2,1)}) custom-call(s32[4]{0:T(128)} %add_add_fusion.2.pos, f32[8,8,256]{2,1,0:T(8,128)} %copy-done, bf16[1,2048]{1,0:T(2,128)(2,1)} %reshape.19.gain, bf16[256,2048]{1,0:T(8,128)(2,1)} %copy-done.7, bf16[256,2048]{1,0:T(8,128)(2,1)} %copy-done.8), custom_call_target="tpu_custom_call" | custom-call | tf_op jit(solution)/shard_map/pick/pallas_call | solution.py:136
  139.4 3.1 %collective-permute-done.20.side = bf16[128,2048]{1,0:T(8,128)(2,1)S(1)} collective-permute-done((bf16[128,2048]{1,0:T(8,128)(2,1)}, bf16[128,2048]{1,0:T(8,128)(2,1)S(1)}, u32[]{:S(2)}, u32[]{:S(2)}) %collective-permute-start.20) | collective-permute-done | bytes 524320 | tf_op jit(solution)/shard_map/ppermute | solution.py:301
  143.2 3.6 %mix.5 = bf16[256,2048]{1,0:T(8,128)(2,1)} custom-call(s32[4]{0:T(128)} %add_add_fusion.3.pos, f32[8,8,256]{2,1,0:T(8,128)} %copy-done, bf16[128,2048]{1,0:T(8,128)(2,1)} %get-tuple-element.31.own, bf16[128,2048]{1,0:T(8,128)(2,1)} %copy-done.10), custom_call_target="tpu_custom_call" | custom-call | tf_op jit(solution)/shard_map/mix/pallas_call | solution.py:245
  146.9 2.4 collective-permute-start.23
  149.3 4.4 %collective-permute-done.3.refs_3_ = bf16[128,2048]{1,0:T(8,128)(2,1)S(1)} collective-permute-done((bf16[128,2048]{1,0:T(8,128)(2,1)}, bf16[128,2048]{1,0:T(8,128)(2,1)S(1)}, u32[]{:S(2)}, u32[]{:S(2)}) %collective-permute-start.3) | collective-permute-done | bytes 524320 | tf_op jit(solution)/shard_map/ppermute | solution.py:301
  153.7 6.4 %collective-permute-done.6.refs_5_ = bf16[128,2048]{1,0:T(8,128)(2,1)S(1)} collective-permute-done((bf16[128,2048]{1,0:T(8,128)(2,1)}, bf16[128,2048]{1,0:T(8,128)(2,1)S(1)}, u32[]{:S(2)}, u32[]{:S(2)}) %collective-permute-start.6) | collective-permute-done | bytes 524320 | tf_op jit(solution)/shard_map/ppermute | solution.py:301
  160.9 17.7 %experts.2 = (bf16[128,2048]{1,0:T(8,128)(2,1)}, bf16[128,2048]{1,0:T(8,128)(2,1)}, bf16[128,2048]{1,0:T(8,128)(2,1)}, bf16[128,2048]{1,0:T(8,128)(2,1)}, bf16[1...) custom-call(bf16[128,2048]{1,0:T(8,128)(2,1)} %get-tuple-element.21.refs_0_, bf16[128,2048]{1,0:T(8,128)(2,1)} %copy-done.15, ...), custom_call_target="tpu_custom_call" | custom-call | flops 9663676416 | bytes 18874368 | tf_op jit(solution)/shard_map/experts/pallas_call | solution.py:198
  179.7 8.4 %collective-permute-done.22.side = bf16[128,2048]{1,0:T(8,128)(2,1)S(1)} collective-permute-done((bf16[128,2048]{1,0:T(8,128)(2,1)}, bf16[128,2048]{1,0:T(8,128)(2,1)S(1)}, u32[]{:S(2)}, u32[]{:S(2)}) %collective-permute-start.22) | collective-permute-done | bytes 524320 | tf_op jit(solution)/shard_map/ppermute | solution.py:301
  189.3 4.1 %mix.7 = bf16[256,2048]{1,0:T(8,128)(2,1)} custom-call(s32[4]{0:T(128)} %add_add_fusion.2.pos, f32[8,8,256]{2,1,0:T(8,128)} %copy-done, bf16[128,2048]{1,0:T(8,128)(2,1)} %get-tuple-element.35.own, bf16[128,2048]{1,0:T(8,128)(2,1)} %copy-done.12, bf16[256,2048]{1,0:T(8,128)(2,1)} %copy-done.9), custom_call_target="tpu_custom_call" | custom-call | tf_op jit(solution)/shard_map/mix/pallas_call | solution.py:245
  194.1 4.0 %collective-permute-start.24 = (bf16[256,2048]{1,0:T(8,128)(2,1)}, bf16[256,2048]{1,0:T(8,128)(2,1)}, u32[]{:S(2)}, u32[]{:S(2)}) collective-permute-start(bf16[256,2048]{1,0:T(8,128)(2,1)} %mix.7), channel_id=1, source_target_pairs={{0,8},{4,12},{8,16},{12,20},{1,9},{5,13},{9,17},{13,21},{2,10},{6,... | collective-permute-start | bytes 3145736 | tf_op jit(solution)/shard_map/ppermute | solution.py:298
  198.8 8.5 %collective-permute-done.21.side = bf16[128,2048]{1,0:T(8,128)(2,1)S(1)} collective-permute-done((bf16[128,2048]{1,0:T(8,128)(2,1)S(1)}, bf16[128,2048]{1,0:T(8,128)(2,1)S(1)}, u32[]{:S(2)}, u32[]{:S(2)}) %collective-permute-start.21) | collective-permute-done | bytes 524320 | tf_op jit(solution)/shard_map/ppermute | solution.py:301
  208.1 3.6 %mix.6 = bf16[256,2048]{1,0:T(8,128)(2,1)} custom-call(s32[4]{0:T(128)} %add_add_fusion.1.pos, f32[8,8,256]{2,1,0:T(8,128)} %copy-done, bf16[128,2048]{1,0:T(8,128)(2,1)} %get-tuple-element.33.own, bf16[128,2048]{1,0:T(8,128)(2,1)} %copy-done.11), custom_call_target="tpu_custom_call" | custom-call | tf_op jit(solution)/shard_map/mix/pallas_call | solution.py:245
  211.8 2.9 %collective-permute-done.24 = bf16[256,2048]{1,0:T(8,128)(2,1)} collective-permute-done((bf16[256,2048]{1,0:T(8,128)(2,1)}, bf16[256,2048]{1,0:T(8,128)(2,1)}, u32[]{:S(2)}, u32[]{:S(2)}) %collective-permute-start.24) | collective-permute-done | bytes 1048608 | tf_op jit(solution)/shard_map/ppermute | solution.py:298
  214.7 3.3 %add_convert_fusion = (bf16[256,2048]{1,0:T(8,128)(2,1)}, bf16[256,2048]{1,0:T(8,128)(2,1)S(1)}) fusion(bf16[256,2048]{1,0:T(8,128)(2,1)S(1)} %collective-permute-done.26, bf16[256,2048]{1,0:T(8,128)(2,1)S(1)} %copy-done.3, bf16[256,2048]{1,0:T(8,128)(2,1)} %mix.6, pred[]{:T(512)S(6)} %eq.13, bf16[256,2048]{1,0:T(8,128)(2,1)} %collective-permute-done.24, ...), kind=kLoop, calls=%fused_computation | loop fusion | flops 5242880 | bytes 6291458 | tf_op jit(solution)/shard_map/convert_element_type | solution.py:364
  219.3 5.1 %collective-permute-start.25 = (bf16[256,2048]{1,0:T(8,128)(2,1)S(1)}, bf16[256,2048]{1,0:T(8,128)(2,1)S(1)}, u32[]{:S(2)}, u32[]{:S(2)}) collective-permute-start(bf16[256,2048]{1,0:T(8,128)(2,1)S(1)} %get-tuple-element.38), channel_id=1, source_target_pairs={{0,8},{4,12},{8,16},{12,20},{16,24},{20,28},{1,9},{5,13},{9,17},{1... | collective-permute-start | bytes 3145736 | tf_op jit(solution)/shard_map/ppermute | solution.py:298
  226.1 6.4 %all_to_all.30 = bf16[4,2,256]{2,1,0:T(2,128)(2,1)S(1)} all-to-all(bf16[4,2,256]{2,1,0:T(2,128)(2,1)S(1)} %reshape.21), channel_id=1, replica_groups=mesh['ep'=8,'tp'=4] {'tp'}, dimensions={0} | all-to-all | bytes 8192 | tf_op jit(solution)/shard_map/all_to_all | solution.py:319
  233.9 4.4 %mix.4.base = f32[256,2048]{1,0:T(8,128)} custom-call(s32[4]{0:T(128)} %add_add_fusion.pos, f32[8,8,256]{2,1,0:T(8,128)} %copy-done, bf16[128,2048]{1,0:T(8,128)(2,1)} %get-tuple-element.27.own, bf16[128,2048]{1,0:T(8,128)(2,1)} %collective-permute-done.16.side, bf16[256,2048]{1,0:T(8,128)(2,1)} %refs_0_.3), custom_call_target="tpu_custom_call" | custom-call | tf_op jit(solution)/shard_map/mix/pallas_call | solution.py:245
  241.6 4.5 %close.1 = bf16[256,2048]{1,0:T(8,128)(2,1)} custom-call(f32[256,2048]{1,0:T(8,128)} %mix.4.base, bf16[256,2048]{1,0:T(8,128)(2,1)} %copy-done.6, bf16[256,2048]{1,0:T(8,128)(2,1)} %copy-done.5, bf16[1,2048]{1,0:T(2,128)(2,1)} %bitcast.23), custom_call_target="tpu_custom_call" | custom-call | tf_op jit(solution)/shard_map/close/pallas_call | solution.py:270
  247.4 17.0 %all_to_all.31 = bf16[256,4,512]{2,0,1:T(8,128)(2,1)S(1)} all-to-all(bf16[256,4,512]{2,0,1:T(8,128)(2,1)S(1)} %bitcast.21), channel_id=1, replica_groups=mesh['ep'=8,'tp'=4] {'tp'}, dimensions={1} | all-to-all | bytes 2097152 | tf_op jit(solution)/shard_map/all_to_all | solution.py:369
  (97 shorter events, 39.2 us)
Async XLA Ops:
  0.0 28.3 %collective-permute-start.1 = (bf16[256,2048]{1,0:T(8,128)(2,1)}, bf16[256,2048]{1,0:T(8,128)(2,1)S(1)}, u32[]{:S(2)}, u32[]{:S(2)}) collective-permute-start(bf16[256,2048]{1,0:T(8,128)(2,1)} %refs_0_.3), channel_id=1, source_target_pairs={{24,16},{28,20},{16,8},{20,12},{8,0},{12,4},{25,17},{29,21},{17,9}... | collective-permute-start | bytes 3145736 | tf_op jit(solution)/shard_map/ppermute | solution.py:298
  1.3 28.3 %collective-permute-start.2 = (bf16[256,2048]{1,0:T(8,128)(2,1)}, bf16[256,2048]{1,0:T(8,128)(2,1)S(1)}, u32[]{:S(2)}, u32[]{:S(2)}) collective-permute-start(bf16[256,2048]{1,0:T(8,128)(2,1)} %refs_0_.3), channel_id=1, source_target_pairs={{0,8},{4,12},{8,16},{12,20},{16,24},{20,28},{1,9},{5,13},{9,17},{1... | collective-permute-start | bytes 3145736 | tf_op jit(solution)/shard_map/ppermute | solution.py:298
  7.0 25.2 %collective-permute-start.8 = (bf16[1,2048,256]{2,1,0:T(8,128)(2,1)}, bf16[1,2048,256]{2,1,0:T(8,128)(2,1)}, u32[]{:S(2)}, u32[]{:S(2)}) collective-permute-start(bf16[1,2048,256]{2,1,0:T(8,128)(2,1)} %refs_2_.1), channel_id=1, source_target_pairs={{0,2},{1,3},{2,0},{3,1},{4,6},{5,7},{6,4},{7,5},{8,10},{9,11},{10,... | collective-permute-start | bytes 3145736 | tf_op jit(solution)/shard_map/ppermute | solution.py:304
  28.3 68.0 %copy-start.1 = (bf16[256,2048]{1,0:T(8,128)(2,1)}, bf16[256,2048]{1,0:T(8,128)(2,1)S(1)}, u32[]{:S(2)}) copy-start(bf16[256,2048]{1,0:T(8,128)(2,1)S(1)} %collective-permute-done.1.refs_0_.refs_2_) | copy-start | bytes 3145732
  28.3 26.3 %collective-permute-start.4 = (bf16[256,2048]{1,0:T(8,128)(2,1)S(1)}, bf16[256,2048]{1,0:T(8,128)(2,1)S(1)}, u32[]{:S(2)}, u32[]{:S(2)}) collective-permute-start(bf16[256,2048]{1,0:T(8,128)(2,1)S(1)} %collective-permute-done.1.refs_0_.refs_2_), channel_id=1, source_target_pairs={{16,8},{20,12},{8,0},{12,4},{17,9},{21,13},{9,1},{13,5},{18,10},{2... | collective-permute-start | bytes 3145736 | tf_op jit(solution)/shard_map/ppermute | solution.py:298
  29.6 66.7 %copy-start.2 = (bf16[256,2048]{1,0:T(8,128)(2,1)}, bf16[256,2048]{1,0:T(8,128)(2,1)S(1)}, u32[]{:S(2)}) copy-start(bf16[256,2048]{1,0:T(8,128)(2,1)S(1)} %collective-permute-done.2.refs_1_) | copy-start | bytes 3145732
  29.6 26.3 %collective-permute-start.5 = (bf16[256,2048]{1,0:T(8,128)(2,1)S(1)}, bf16[256,2048]{1,0:T(8,128)(2,1)S(1)}, u32[]{:S(2)}, u32[]{:S(2)}) collective-permute-start(bf16[256,2048]{1,0:T(8,128)(2,1)S(1)} %collective-permute-done.2.refs_1_), channel_id=1, source_target_pairs={{8,16},{12,20},{16,24},{20,28},{9,17},{13,21},{17,25},{21,29},{10,... | collective-permute-start | bytes 3145736 | tf_op jit(solution)/shard_map/ppermute | solution.py:298
  30.4 27.2 %collective-permute-start.7 = (bf16[1,2048,256]{2,1,0:T(8,128)(2,1)}, bf16[1,2048,256]{2,1,0:T(8,128)(2,1)}, u32[]{:S(2)}, u32[]{:S(2)}) collective-permute-start(bf16[1,2048,256]{2,1,0:T(8,128)(2,1)} %refs_2_.1), channel_id=1, source_target_pairs={{0,1},{1,0},{2,3},{3,2},{4,5},{5,4},{6,7},{7,6},{8,9},{9,8},{10,11... | collective-permute-start | bytes 3145736 | tf_op jit(solution)/shard_map/ppermute | solution.py:304
  30.4 28.7 %collective-permute-start.11 = (bf16[1,2048,256]{2,1,0:T(8,128)(2,1)}, bf16[1,2048,256]{2,1,0:T(8,128)(2,1)}, u32[]{:S(2)}, u32[]{:S(2)}) collective-permute-start(bf16[1,2048,256]{2,1,0:T(8,128)(2,1)} %refs_6_.3), channel_id=1, source_target_pairs={{0,2},{1,3},{2,0},{3,1},{4,6},{5,7},{6,4},{7,5},{8,10},{9,11},{10,... | collective-permute-start | bytes 3145736 | tf_op jit(solution)/shard_map/ppermute | solution.py:304
  32.2 46.6 %collective-permute-start.14 = (bf16[1,256,2048]{2,1,0:T(8,128)(2,1)}, bf16[1,256,2048]{2,1,0:T(8,128)(2,1)}, u32[]{:S(2)}, u32[]{:S(2)}) collective-permute-start(bf16[1,256,2048]{2,1,0:T(8,128)(2,1)} %refs_10_.3), channel_id=1, source_target_pairs={{0,2},{1,3},{2,0},{3,1},{4,6},{5,7},{6,4},{7,5},{8,10},{9,11},{10,... | collective-permute-start | bytes 3145736 | tf_op jit(solution)/shard_map/ppermute | solution.py:304
  54.6 25.6 %copy-start.7 = (bf16[256,2048]{1,0:T(8,128)(2,1)}, bf16[256,2048]{1,0:T(8,128)(2,1)S(1)}, u32[]{:S(2)}) copy-start(bf16[256,2048]{1,0:T(8,128)(2,1)S(1)} %collective-permute-done.4.refs_0_) | copy-start | bytes 3145732
  54.6 25.6 %collective-permute-start.17 = (bf16[256,2048]{1,0:T(8,128)(2,1)S(1)}, bf16[256,2048]{1,0:T(8,128)(2,1)S(1)}, u32[]{:S(2)}, u32[]{:S(2)}) collective-permute-start(bf16[256,2048]{1,0:T(8,128)(2,1)S(1)} %collective-permute-done.4.refs_0_), channel_id=1, source_target_pairs={{8,0},{12,4},{9,1},{13,5},{10,2},{14,6},{11,3},{15,7}} | collective-permute-start | bytes 3145736 | tf_op jit(solution)/shard_map/ppermute | solution.py:298
  55.9 24.3 %collective-permute-start.18 = (bf16[256,2048]{1,0:T(8,128)(2,1)S(1)}, bf16[256,2048]{1,0:T(8,128)(2,1)}, u32[]{:S(2)}, u32[]{:S(2)}) collective-permute-start(bf16[256,2048]{1,0:T(8,128)(2,1)S(1)} %collective-permute-done.5.refs_1_), channel_id=1, source_target_pairs={{16,24},{20,28},{17,25},{21,29},{18,26},{22,30},{19,27},{23,31}} | collective-permute-start | bytes 3145736 | tf_op jit(solution)/shard_map/ppermute | solution.py:298
  57.6 44.1 %collective-permute-start.10 = (bf16[1,2048,256]{2,1,0:T(8,128)(2,1)}, bf16[1,2048,256]{2,1,0:T(8,128)(2,1)}, u32[]{:S(2)}, u32[]{:S(2)}) collective-permute-start(bf16[1,2048,256]{2,1,0:T(8,128)(2,1)} %refs_6_.3), channel_id=1, source_target_pairs={{0,1},{1,0},{2,3},{3,2},{4,5},{5,4},{6,7},{7,6},{8,9},{9,8},{10,11... | collective-permute-start | bytes 3145736 | tf_op jit(solution)/shard_map/ppermute | solution.py:304
  59.1 49.6 %collective-permute-start.13 = (bf16[1,256,2048]{2,1,0:T(8,128)(2,1)}, bf16[1,256,2048]{2,1,0:T(8,128)(2,1)}, u32[]{:S(2)}, u32[]{:S(2)}) collective-permute-start(bf16[1,256,2048]{2,1,0:T(8,128)(2,1)} %refs_10_.3), channel_id=1, source_target_pairs={{0,1},{1,0},{2,3},{3,2},{4,5},{5,4},{6,7},{7,6},{8,9},{9,8},{10,11... | collective-permute-start | bytes 3145736 | tf_op jit(solution)/shard_map/ppermute | solution.py:304
  78.8 31.6 %collective-permute-start.9 = (bf16[1,2048,256]{2,1,0:T(8,128)(2,1)}, bf16[1,2048,256]{2,1,0:T(8,128)(2,1)}, u32[]{:S(2)}, u32[]{:S(2)}) collective-permute-start(bf16[1,2048,256]{2,1,0:T(8,128)(2,1)} %collective-permute-done.8.refs_8_.refs_4_), channel_id=1, source_target_pairs={{0,1},{1,0},{2,3},{3,2},{4,5},{5,4},{6,7},{7,6},{8,9},{9,8},{10,11... | collective-permute-start | bytes 3145736 | tf_op jit(solution)/shard_map/ppermute | solution.py:304
  80.2 30.2 %collective-permute-start.12 = (bf16[1,2048,256]{2,1,0:T(8,128)(2,1)}, bf16[1,2048,256]{2,1,0:T(8,128)(2,1)}, u32[]{:S(2)}, u32[]{:S(2)}) collective-permute-start(bf16[1,2048,256]{2,1,0:T(8,128)(2,1)} %collective-permute-done.11.refs_12_.refs_8_), channel_id=1, source_target_pairs={{0,1},{1,0},{2,3},{3,2},{4,5},{5,4},{6,7},{7,6},{8,9},{9,8},{10,11... | collective-permute-start | bytes 3145736 | tf_op jit(solution)/shard_map/ppermute | solution.py:304
  80.2 30.2 %collective-permute-start.15 = (bf16[1,256,2048]{2,1,0:T(8,128)(2,1)}, bf16[1,256,2048]{2,1,0:T(8,128)(2,1)}, u32[]{:S(2)}, u32[]{:S(2)}) collective-permute-start(bf16[1,256,2048]{2,1,0:T(8,128)(2,1)} %collective-permute-done.14.refs_16_.refs_12_), channel_id=1, source_target_pairs={{0,1},{1,0},{2,3},{3,2},{4,5},{5,4},{6,7},{7,6},{8,9},{9,8},{10,11... | collective-permute-start | bytes 3145736 | tf_op jit(solution)/shard_map/ppermute | solution.py:304
  82.1 14.2 %all-to-all-start = ((f32[8,8,256]{2,1,0:T(8,128)}), f32[8,8,256]{2,1,0:T(8,128)S(1)}, u32[]{:S(2)}, u32[]{:S(2)}) async-start(f32[8,8,256]{2,1,0:T(8,128)} %broadcast_in_dim.7), calls=%async_computation | async-start | bytes 131072 | tf_op jit(solution)/shard_map/all_to_all | solution.py:316
  101.7 15.1 %collective-permute-start.19 = (bf16[128,2048]{1,0:T(8,128)(2,1)}, bf16[128,2048]{1,0:T(8,128)(2,1)S(1)}, u32[]{:S(2)}, u32[]{:S(2)}) collective-permute-start(bf16[128,2048]{1,0:T(8,128)(2,1)} %get-tuple-element.30), channel_id=1, source_target_pairs={{0,4},{4,0},{8,12},{12,8},{16,20},{20,16},{24,28},{28,24},{1,5},{5... | collective-permute-start | bytes 1572872 | tf_op jit(solution)/shard_map/ppermute | solution.py:301
  108.7 40.6 %collective-permute-start = (bf16[128,2048]{1,0:T(8,128)(2,1)}, bf16[128,2048]{1,0:T(8,128)(2,1)S(1)}, u32[]{:S(2)}, u32[]{:S(2)}) collective-permute-start(bf16[128,2048]{1,0:T(8,128)(2,1)} %get-tuple-element.22), channel_id=1, source_target_pairs={{0,4},{4,0},{8,12},{12,8},{16,20},{20,16},{24,28},{28,24},{1,5},{5... | collective-permute-start | bytes 1572872 | tf_op jit(solution)/shard_map/ppermute | solution.py:301
  127.4 15.1 %collective-permute-start.20 = (bf16[128,2048]{1,0:T(8,128)(2,1)}, bf16[128,2048]{1,0:T(8,128)(2,1)S(1)}, u32[]{:S(2)}, u32[]{:S(2)}) collective-permute-start(bf16[128,2048]{1,0:T(8,128)(2,1)} %get-tuple-element.32), channel_id=1, source_target_pairs={{0,4},{4,0},{8,12},{12,8},{16,20},{20,16},{24,28},{28,24},{1,5},{5... | collective-permute-start | bytes 1572872 | tf_op jit(solution)/shard_map/ppermute | solution.py:301
  132.5 21.2 %collective-permute-start.3 = (bf16[128,2048]{1,0:T(8,128)(2,1)}, bf16[128,2048]{1,0:T(8,128)(2,1)S(1)}, u32[]{:S(2)}, u32[]{:S(2)}) collective-permute-start(bf16[128,2048]{1,0:T(8,128)(2,1)} %get-tuple-element.24), channel_id=1, source_target_pairs={{0,4},{4,0},{8,12},{12,8},{16,20},{20,16},{24,28},{28,24},{1,5},{5... | collective-permute-start | bytes 1572872 | tf_op jit(solution)/shard_map/ppermute | solution.py:301
  138.9 21.2 %collective-permute-start.6 = (bf16[128,2048]{1,0:T(8,128)(2,1)}, bf16[128,2048]{1,0:T(8,128)(2,1)S(1)}, u32[]{:S(2)}, u32[]{:S(2)}) collective-permute-start(bf16[128,2048]{1,0:T(8,128)(2,1)} %get-tuple-element.26), channel_id=1, source_target_pairs={{0,4},{4,0},{8,12},{12,8},{16,20},{20,16},{24,28},{28,24},{1,5},{5... | collective-permute-start | bytes 1572872 | tf_op jit(solution)/shard_map/ppermute | solution.py:301
  146.9 41.3 %collective-permute-start.23 = (bf16[256,2048]{1,0:T(8,128)(2,1)}, bf16[256,2048]{1,0:T(8,128)(2,1)S(1)}, u32[]{:S(2)}, u32[]{:S(2)}) collective-permute-start(bf16[256,2048]{1,0:T(8,128)(2,1)} %mix.5), channel_id=1, source_target_pairs={{0,8},{4,12},{24,16},{28,20},{1,9},{5,13},{25,17},{29,21},{2,10},{... | collective-permute-start | bytes 3145736 | tf_op jit(solution)/shard_map/ppermute | solution.py:298
  178.7 9.5 %collective-permute-start.22 = (bf16[128,2048]{1,0:T(8,128)(2,1)}, bf16[128,2048]{1,0:T(8,128)(2,1)S(1)}, u32[]{:S(2)}, u32[]{:S(2)}) collective-permute-start(bf16[128,2048]{1,0:T(8,128)(2,1)} %get-tuple-element.36), channel_id=1, source_target_pairs={{0,4},{4,0},{8,12},{12,8},{16,20},{20,16},{24,28},{28,24},{1,5},{5... | collective-permute-start | bytes 1572872 | tf_op jit(solution)/shard_map/ppermute | solution.py:301
  193.4 18.4 %collective-permute-start.26 = (bf16[256,2048]{1,0:T(8,128)(2,1)}, bf16[256,2048]{1,0:T(8,128)(2,1)S(1)}, u32[]{:S(2)}, u32[]{:S(2)}) collective-permute-start(bf16[256,2048]{1,0:T(8,128)(2,1)} %mix.7), channel_id=1, source_target_pairs={{24,16},{28,20},{16,8},{20,12},{25,17},{29,21},{17,9},{21,13},{26,... | collective-permute-start | bytes 3145736 | tf_op jit(solution)/shard_map/ppermute | solution.py:298
  194.1 20.6 %collective-permute-start.24 = (bf16[256,2048]{1,0:T(8,128)(2,1)}, bf16[256,2048]{1,0:T(8,128)(2,1)}, u32[]{:S(2)}, u32[]{:S(2)}) collective-permute-start(bf16[256,2048]{1,0:T(8,128)(2,1)} %mix.7), channel_id=1, source_target_pairs={{0,8},{4,12},{8,16},{12,20},{1,9},{5,13},{9,17},{13,21},{2,10},{6,... | collective-permute-start | bytes 3145736 | tf_op jit(solution)/shard_map/ppermute | solution.py:298
  198.1 9.2 %collective-permute-start.21 = (bf16[128,2048]{1,0:T(8,128)(2,1)S(1)}, bf16[128,2048]{1,0:T(8,128)(2,1)S(1)}, u32[]{:S(2)}, u32[]{:S(2)}) collective-permute-start(bf16[128,2048]{1,0:T(8,128)(2,1)S(1)} %copy-done.17), channel_id=1, source_target_pairs={{0,4},{4,0},{8,12},{12,8},{16,20},{20,16},{24,28},{28,24},{1,5},{5... | collective-permute-start | bytes 1572872 | tf_op jit(solution)/shard_map/ppermute | solution.py:301
  218.0 21.7 %collective-permute-start.27 = (bf16[256,2048]{1,0:T(8,128)(2,1)}, bf16[256,2048]{1,0:T(8,128)(2,1)S(1)}, u32[]{:S(2)}, u32[]{:S(2)}) collective-permute-start(bf16[256,2048]{1,0:T(8,128)(2,1)} %get-tuple-element.37), channel_id=1, source_target_pairs={{24,16},{28,20},{16,8},{20,12},{8,0},{12,4},{25,17},{29,21},{17,9}... | collective-permute-start | bytes 3145736 | tf_op jit(solution)/shard_map/ppermute | solution.py:298
  219.3 21.4 %collective-permute-start.25 = (bf16[256,2048]{1,0:T(8,128)(2,1)S(1)}, bf16[256,2048]{1,0:T(8,128)(2,1)S(1)}, u32[]{:S(2)}, u32[]{:S(2)}) collective-permute-start(bf16[256,2048]{1,0:T(8,128)(2,1)S(1)} %get-tuple-element.38), channel_id=1, source_target_pairs={{0,8},{4,12},{8,16},{12,20},{16,24},{20,28},{1,9},{5,13},{9,17},{1... | collective-permute-start | bytes 3145736 | tf_op jit(solution)/shard_map/ppermute | solution.py:298
  224.4 9.6 %collective-permute-start.16 = (bf16[128,2048]{1,0:T(8,128)(2,1)}, bf16[128,2048]{1,0:T(8,128)(2,1)}, u32[]{:S(2)}, u32[]{:S(2)}) collective-permute-start(bf16[128,2048]{1,0:T(8,128)(2,1)} %get-tuple-element.28), channel_id=1, source_target_pairs={{0,4},{4,0},{8,12},{12,8},{16,20},{20,16},{24,28},{28,24},{1,5},{5... | collective-permute-start | bytes 1572872 | tf_op jit(solution)/shard_map/ppermute | solution.py:301
  (16 other events, 123.5 us)
